TPU v7x, 256 devices: a 4x2x16 block of a 4x16x16 slice. The times are simulated.
256 devices in a mesh: grp: 2 (over y), ep: 32 (over z, core), tp: 4 (over x).
Axes of the slice: x: 4, y: 2, z: 16, core: 2. Of those that a mesh axis runs over, the one named last changes fastest.
The devices are a block of a 4x16x16 slice.
Arguments:
- mixer_tokens: bfloat16 [32768, 2048], P(('grp', 'ep', 'tp')), parts along dimension 0, may hold values from -6 to 6
- mixer_gain: bfloat16 [2048], replicated, may hold values from 0.099609375 to 1.8984375
- in_weight: bfloat16 [2048, 2048], P(None, 'tp'), may hold values from -0.125 to 0.125
- group_weight: bfloat16 [4, 512, 512], P('tp'), may hold values from -0.25 to 0.25
- channel_scale: bfloat16 [2048], P('tp'), may hold values from 0.099609375 to 1.8984375
- out_weight: bfloat16 [2048, 2048], P('tp'), may hold values from -0.125 to 0.125
- expert_tokens: bfloat16 [32768, 2048], P(('grp', 'ep', 'tp')), parts along dimension 0, may hold values from -6 to 6
- expert_gain: bfloat16 [2048], replicated, may hold values from 0.099609375 to 1.8984375
- route_ids: int32 [32768, 2], P(('grp', 'ep', 'tp')), parts along dimension 0, may hold values from 0 to 31, all different within a row; in each aligned block of 128 rows (0 to 127, 128 to 255, ...) at most 16 rows name the same one
- route_weights: float32 [32768, 2], P(('grp', 'ep', 'tp')), parts along dimension 0, may hold values from 0.1 to 1
- gate_weight: bfloat16 [32, 2048, 1024], P('ep', None, 'tp'), may hold values from -0.125 to 0.125
- up_weight: bfloat16 [32, 2048, 1024], P('ep', None, 'tp'), may hold values from -0.125 to 0.125
- down_weight: bfloat16 [32, 1024, 2048], P('ep', 'tp'), may hold values from -0.1875 to 0.1875
Outputs:
- mixed_tokens: bfloat16 [32768, 2048], P(('grp', 'ep', 'tp')), parts along dimension 0
- expert_mix: bfloat16 [32768, 2048], P(('grp', 'ep', 'tp')), parts along dimension 0
There are 2 independent parts, one for each index of `grp`. A program takes and returns all parts, laid end to end along the dimension named above; an argument that names none is the same for every part. Nothing has to cross between parts.
Inputs may be any that keep to these rules, and one draw needn't show every extreme that they name: `route_ids`: each row names 2 different experts; in the rows of one device no expert is named more than 16 times, and one expert exactly 16 times in the rows of some device.
All inputs are finite; a program needn't handle non-finite values.
Results may differ from a plain program's by a relative error of at most 0.015.
Values may be sent and summed in bfloat16 or wider, within the bound.
No kernel may reach another device: no remote copies, remote signals or barrier semaphores. Data moves between devices by JAX's collectives and lax.ppermute only.
A program may use at most 128 MiB of HBM per device.

v0:
```python
import jax
import jax.numpy as jnp
from jax import lax
from jax.sharding import PartitionSpec as P

WINDOW_MAX = 16


def from_everyone(value, axis):
    devices = lax.axis_size(axis)
    return lax.all_to_all(
        jnp.broadcast_to(value[None], (devices, *value.shape)), axis, 0, 0, tiled=True
    )


def joined_along(tiles, dim):
    tiles = jnp.moveaxis(tiles, 0, dim)
    shape = tiles.shape
    return tiles.reshape(*shape[:dim], shape[dim] * shape[dim + 1], *shape[dim + 2 :])


def collect(value, axis, dim):
    tiles = from_everyone(value, axis)
    return joined_along(tiles, dim)


def shifted(value, axis, by):
    devices = lax.axis_size(axis)
    pairs = [(i, i + by) for i in range(devices) if 0 <= i + by < devices]
    return lax.ppermute(value, axis, pairs)


def cut_along(value, dim, devices):
    shape = value.shape
    tiles = value.reshape(*shape[:dim], devices, shape[dim] // devices, *shape[dim + 1 :])
    return jnp.moveaxis(tiles, dim, 0)


def sent_and_summed(value, axis, dim):
    tiles = cut_along(value, dim, lax.axis_size(axis))
    arrived = lax.all_to_all(tiles, axis, split_axis=0, concat_axis=0, tiled=True)
    return arrived.astype(jnp.float32).sum(axis=0)


def exchange_in_groups(value, axis, split_dim, concat_dim, work, item_dim, out_dim):

    def moved(group):
        return lax.all_to_all(group, axis, split_axis=split_dim, concat_axis=concat_dim, tiled=True)

    items = jax.tree.leaves(value)[0].shape[item_dim]
    ends = [items * k // 2 for k in range(2 + 1)] if items % 2 == 0 else [0, items]
    groups = [
        jax.tree.map(lambda a: lax.slice_in_dim(a, low, high, axis=item_dim), value)
        for low, high in zip(ends, ends[1:])
    ]
    arrived = [moved(group) for group in groups]
    made = [work(group) for group in arrived]
    return jax.tree.map(lambda *parts: jnp.concatenate(parts, axis=out_dim), *made)


def rms_rows(rows, gain):
    values = rows.astype(jnp.float32)
    scaled = values * lax.rsqrt(jnp.mean(values * values, axis=-1, keepdims=True) + 1e-06)
    return (scaled * gain.astype(jnp.float32)).astype(jnp.bfloat16)


def expert_hidden(rows, w_gate, w_up):
    gate = jnp.dot(rows, w_gate, preferred_element_type=jnp.float32)
    upper = jnp.dot(rows, w_up, preferred_element_type=jnp.float32)
    return (jax.nn.silu(gate) * upper).astype(jnp.bfloat16)


def local(
    mixer_tokens,
    mixer_gain,
    in_weight,
    group_weight,
    channel_scale,
    out_weight,
    expert_tokens,
    expert_gain,
    route_ids,
    route_weights,
    gate_weight,
    up_weight,
    down_weight,
):
    normed = rms_rows(mixer_tokens, mixer_gain)
    pooled_in = jnp.dot(
        collect(normed, "tp", 0), in_weight, preferred_element_type=jnp.float32
    ).astype(jnp.bfloat16)
    block_rows = pooled_in.shape[0]
    rim_rows = shifted(pooled_in[block_rows - WINDOW_MAX :], "ep", 1)
    values = pooled_in.astype(jnp.float32)
    extended = jnp.concatenate([rim_rows.astype(jnp.float32), values], axis=0)
    window = jnp.left_shift(jnp.int32(2), lax.axis_index("tp"))
    sums = extended
    span = 1
    total = jnp.zeros_like(values)
    for level in range(WINDOW_MAX.bit_length() - 1):
        sums = sums[span:] + sums[:-span]
        span = span * 2
        total = total + jnp.where(window == span, sums[sums.shape[0] - block_rows :], 0.0)
    positions = lax.axis_index("ep") * block_rows + lax.iota(jnp.int32, block_rows) + 1
    counts = jnp.minimum(positions, window).astype(jnp.float32)
    pooled = (total / counts[:, None] - values).astype(jnp.bfloat16)
    grouped = (
        jnp.dot(pooled, group_weight[0], preferred_element_type=jnp.float32)
        * channel_scale.astype(jnp.float32)
    ).astype(jnp.bfloat16)
    rows = grouped
    mixed_tokens = sent_and_summed(
        jnp.dot(rows, out_weight, preferred_element_type=jnp.float32).astype(jnp.bfloat16), "tp", 0
    ).astype(jnp.bfloat16)
    expert_in = rms_rows(expert_tokens, expert_gain)
    shares = route_weights / jnp.sum(route_weights, axis=1, keepdims=True)
    rows_here, top_k = route_ids.shape
    width = expert_in.shape[1]
    n_experts = lax.axis_size("ep") * gate_weight.shape[0]
    capacity = 4 * rows_here // n_experts
    flat_ids = route_ids.reshape(rows_here * top_k)
    one_hot = (flat_ids[:, None] == jnp.arange(n_experts, dtype=jnp.int32)[None, :]).astype(
        jnp.int32
    )
    before = jnp.cumsum(one_hot, axis=0) - one_hot
    slots = jnp.sum(before * one_hot, axis=1)
    targets = flat_ids * capacity + slots
    placement = (
        targets.reshape(rows_here, top_k)[None, :, :]
        == jnp.arange(n_experts * capacity, dtype=jnp.int32)[:, None, None]
    )
    dispatch = jnp.any(placement, axis=2).astype(jnp.bfloat16)
    outgoing = jnp.dot(dispatch, expert_in, preferred_element_type=jnp.float32).astype(jnp.bfloat16)
    outgoing = outgoing.reshape(n_experts, capacity, width)

    def serve_sectioned(arrived):
        sources, held, _ = arrived.shape
        flat = arrived.reshape(sources * held, width)
        hidden = expert_hidden(
            lax.all_gather(flat, "tp", axis=0, tiled=True), gate_weight[0], up_weight[0]
        )
        rows = lax.slice_in_dim(hidden, 0, sources * held * lax.axis_size("tp"), axis=0)
        summed = lax.psum_scatter(
            jnp.dot(rows, down_weight[0], preferred_element_type=jnp.float32).astype(jnp.bfloat16),
            "tp",
            scatter_dimension=0,
            tiled=True,
        ).astype(jnp.float32)
        return lax.all_to_all(
            summed.reshape(sources, held, width).astype(jnp.bfloat16),
            "ep",
            split_axis=0,
            concat_axis=0,
            tiled=True,
        ).astype(jnp.float32)

    expert_out = exchange_in_groups(outgoing, "ep", 0, 0, serve_sectioned, 1, 1)
    flat_out = expert_out.reshape(n_experts * capacity, width)
    picked = jnp.take(flat_out, targets, axis=0).reshape(rows_here, top_k, width)
    expert_mix = jnp.sum(picked * shares[:, :, None], axis=1).astype(jnp.bfloat16)
    return (mixed_tokens, expert_mix)


def solution(mesh):
    placed = (
        P(("grp", "ep", "tp"), None),
        P(),
        P(None, "tp"),
        P("tp", None, None),
        P("tp"),
        P("tp", None),
        P(("grp", "ep", "tp"), None),
        P(),
        P(("grp", "ep", "tp"), None),
        P(("grp", "ep", "tp"), None),
        P("ep", None, "tp"),
        P("ep", None, "tp"),
        P("ep", "tp", None),
    )
    return jax.shard_map(
        local,
        mesh=mesh,
        in_specs=placed,
        out_specs=(P(("grp", "ep", "tp"), None), P(("grp", "ep", "tp"), None)),
        check_vma=False,
    )
```

profile of v0, /device:TPU:33, one launch (start us, length us, event | category | flops | bytes accessed | tf_op | source)
XLA Modules:
  0.0 458.0 jit_solution(7608851029754211037)
XLA Ops:
  7.2 0.0 copy-start
  7.2 0.1 all-gather.3.cloned.1.call-start
  7.3 0.9 copy.29
  8.2 0.1 eq.55
  8.3 0.1 reshape.128
  8.5 0.6 reduce-window.6
  9.1 0.2 slice_reduce_fusion
  9.3 0.1 fusion.64
  9.4 0.1 reduce_sum.64
  9.6 0.1 copy.32
  9.6 0.7 compare_and_fusion
  10.3 0.1 fusion.51
  10.4 0.7 convert_element_type.100
  11.1 1.2 fusion.7
  12.3 1.8 convolution_convert_fusion.2
  14.1 0.2 fusion.72
  14.3 80.9 %all_to_all.30 = bf16[32,8,2048]{2,1,0:T(8,128)(2,1)} all-to-all(bf16[32,8,2048]{2,1,0:T(8,128)(2,1)S(1)} %get-tuple-element.4), channel_id=1, replica_groups=mesh['grp'=2,'ep'=32,'tp'=4] {'ep'}, dimensions={0} | all-to-all | bytes 2097152 | tf_op jit(solution)/shard_map/all_to_all | solution.py:48
  95.2 0.1 all-gather.3.cloned.1.call-update
  95.3 0.1 all-gather.5.cloned.1.call-start
  95.3 59.7 %all_to_all.31 = bf16[32,8,2048]{2,1,0:T(8,128)(2,1)} all-to-all(bf16[32,8,2048]{2,1,0:T(8,128)(2,1)S(1)} %get-tuple-element.5), channel_id=1, replica_groups=mesh['grp'=2,'ep'=32,'tp'=4] {'ep'}, dimensions={0} | all-to-all | bytes 2097152 | tf_op jit(solution)/shard_map/all_to_all | solution.py:48
  155.0 0.1 all-gather.5.cloned.1.call-update
  155.1 0.0 copy-start.10
  155.1 0.1 reduce-scatter.3.cloned.1.call-start
  155.2 0.0 all-gather.3.cloned.1.call-done
  155.2 4.9 %fusion.24 = f32[1024,256]{1,0:T(8,128)} fusion(bf16[1024,2048]{1,0:T(8,128)(2,1)} %all-gather.3.cloned.1.call-done, bf16[1,2048,256]{2,1,0:T(8,128)(2,1)} %param.23), kind=kOutput, calls=%fused_computation.45 | convolution fusion | flops 1073741824 | bytes 6291456 | tf_op jit(solution)/shard_map/dot_general | solution.py:68
  160.0 9.2 %convolution_convert_fusion.1 = bf16[1024,2048]{1,0:T(8,128)(2,1)} fusion(bf16[1024,2048]{1,0:T(8,128)(2,1)} %all-gather.3.cloned.1.call-done, bf16[1,256,2048]{2,1,0:T(8,128)(2,1)S(1)} %copy-done.10, bf16[1,2048,256]{2,1,0:T(8,128)(2,1)} %param.24, f32[1024,256]{1,0:T(8,128)} %fusion.24), kind=kOutput, calls=%fused_computation.2 | convolution fusion | flops 2151153664 | bytes 11534336 | tf_op jit(solution)/shard_map/dot_general | solution.py:144
  169.2 0.1 reduce-scatter.3.cloned.1.call-update
  169.3 0.6 copy-done.5
  169.9 0.4 copy-done.3
  170.2 0.2 fusion.4
  170.4 0.2 fusion.6
  170.7 1.6 broadcast_in_dim.16
  172.2 4.7 %all-to-all-start = ((bf16[4,128,2048]{2,1,0:T(8,128)(2,1)}), bf16[4,128,2048]{2,1,0:T(8,128)(2,1)}, u32[]{:S(2)}, u32[]{:S(2)}) async-start(bf16[4,128,2048]{2,1,0:T(8,128)(2,1)} %broadcast_in_dim.16), calls=%async_computation | async-start | bytes 4194304 | tf_op jit(solution)/shard_map/all_to_all | solution.py:11
  177.0 0.2 reduce-scatter.5.cloned.1.call-start
  177.2 44.4 %all-gather.5.cloned.1.call-done = bf16[1024,2048]{1,0:T(8,128)(2,1)} async-done(((bf16[256,2048]{1,0:T(8,128)(2,1)}), bf16[1024,2048]{1,0:T(8,128)(2,1)}) %all-gather.5.cloned.1.call-update) | async-done | bytes 4194320 | tf_op jit(solution)/shard_map/all_gather | solution.py:140
  221.6 4.5 fusion.22
  226.1 9.4 %convolution_convert_fusion = bf16[1024,2048]{1,0:T(8,128)(2,1)} fusion(bf16[1024,2048]{1,0:T(8,128)(2,1)} %all-gather.5.cloned.1.call-done, bf16[1,256,2048]{2,1,0:T(8,128)(2,1)} %param.25, bf16[1,2048,256]{2,1,0:T(8,128)(2,1)} %param.24, f32[1024,256]{1,0:T(8,128)} %fusion.22), kind=kOutput, calls=%fused_computation.1 | convolution fusion | flops 2151153664 | bytes 11534336 | tf_op jit(solution)/shard_map/dot_general | solution.py:144
  235.5 0.1 reduce-scatter.5.cloned.1.call-update
  235.6 0.0 copy-start.7
  235.6 4.5 fusion.74
  240.0 6.5 %collective-permute-start = (bf16[16,512]{1,0:T(8,128)(2,1)S(1)}, bf16[16,512]{1,0:T(8,128)(2,1)S(1)}, u32[]{:S(2)}, u32[]{:S(2)}) collective-permute-start(bf16[16,512]{1,0:T(8,128)(2,1)S(1)} %slice.70), channel_id=1, source_target_pairs={{0,4},{4,8},{8,12},{12,16},{16,20},{20,24},{24,28},{28,32},{32,36}... | collective-permute-start | bytes 49160 | tf_op jit(solution)/shard_map/ppermute | solution.py:30
  246.6 0.8 collective-permute-done
  247.4 1.8 fusion.3
  249.2 0.1 slice_add_fusion.1
  249.4 1.0 copy-done.1
  250.3 0.1 slice_add_fusion
  250.5 1.7 fusion.73
  252.2 5.9 %convolution_convert_fusion.3 = bf16[512,2048]{1,0:T(8,128)(2,1)} fusion(bf16[512,2048]{1,0:T(8,128)(2,1)S(1)} %copy-done, f32[513,512]{1,0:T(8,128)} %get-tuple-element.7, f32[513,512]{1,0:T(8,128)} %get-tuple-element.6, f32[521,512]{1,0:T(8,128)} %copy-done.2, f32[525,512]{1,0:T(8,128)} %copy-done.1, f32[527,512]{1,0:T(8,128)S(1)} %fusion.3, ...), kind=kOutput, calls=%fused_computation.4 | convolution fusion | flops 1346895872 | bytes 10489860 | tf_op jit(solution)/shard_map/dot_general | solution.py:113
  258.1 43.6 %all_to_all.32 = bf16[4,128,2048]{2,1,0:T(8,128)(2,1)} all-to-all(bf16[4,128,2048]{2,1,0:T(8,128)(2,1)} %bitcast.63), channel_id=1, replica_groups=mesh['grp'=2,'ep'=32,'tp'=4] {'tp'}, dimensions={0} | all-to-all | bytes 4194304 | tf_op jit(solution)/shard_map/all_to_all | solution.py:41
  301.7 13.9 %all-to-all-start.3 = ((bf16[32,8,2048]{2,1,0:T(8,128)(2,1)}), bf16[32,8,2048]{2,1,0:T(8,128)(2,1)S(1)}, u32[]{:S(2)}, u32[]{:S(2)}) async-start(bf16[32,8,2048]{2,1,0:T(8,128)(2,1)} %bitcast.64), calls=%async_computation.4 | async-start | bytes 2097152 | tf_op jit(solution)/shard_map/all_to_all | solution.py:149
  315.7 41.5 %reduce-scatter.5.cloned.1.call-done = bf16[256,2048]{1,0:T(8,128)(2,1)} async-done(((bf16[1024,2048]{1,0:T(8,128)(2,1)}), bf16[256,2048]{1,0:T(8,128)(2,1)}) %reduce-scatter.5.cloned.1.call-update) | async-done | bytes 1048592 | tf_op jit(solution)/shard_map/reduce_scatter | solution.py:143
  357.2 13.9 %all-to-all-done.3 = bf16[32,8,2048]{2,1,0:T(8,128)(2,1)S(1)} async-done(((bf16[32,8,2048]{2,1,0:T(8,128)(2,1)}), bf16[32,8,2048]{2,1,0:T(8,128)(2,1)S(1)}, u32[]{:S(2)}, u32[]{:S(2)}) %all-to-all-start.3) | async-done | bytes 1048608 | tf_op jit(solution)/shard_map/all_to_all | solution.py:149
  371.2 5.1 %all-to-all-start.5 = ((bf16[32,8,2048]{2,1,0:T(8,128)(2,1)}), bf16[32,8,2048]{2,1,0:T(8,128)(2,1)}, u32[]{:S(2)}, u32[]{:S(2)}) async-start(bf16[32,8,2048]{2,1,0:T(8,128)(2,1)} %bitcast.65), calls=%async_computation.7 | async-start | bytes 2097152 | tf_op jit(solution)/shard_map/all_to_all | solution.py:149
  376.3 0.1 copy.34
  376.4 0.1 mul.114
  376.5 0.1 copy.33
  376.7 0.1 copy.35
  376.9 2.9 reduce_sum.62
  379.8 52.0 %all-to-all-done.5 = bf16[32,8,2048]{2,1,0:T(8,128)(2,1)} async-done(((bf16[32,8,2048]{2,1,0:T(8,128)(2,1)}), bf16[32,8,2048]{2,1,0:T(8,128)(2,1)}, u32[]{:S(2)}, u32[]{:S(2)}) %all-to-all-start.5) | async-done | bytes 1048608 | tf_op jit(solution)/shard_map/all_to_all | solution.py:149
  431.8 1.4 pad_maximum_fusion
  433.2 2.6 bitcast_convert_fusion
  435.8 5.8 %gather_fusion = f32[256,2048]{1,0:T(8,128)} fusion(f32[512,2048]{1,0:T(8,128)} %bitcast_convert_fusion, s32[1024]{0:T(1024)S(1)} %pad_clamp_fusion), kind=kCustom, calls=%fused_computation | custom fusion | bytes 4195328 | tf_op jit(solution)/shard_map/jit(_take)/gather | solution.py:159
  441.6 3.5 gather.7
  445.1 6.4 %multiply_reduce_fusion = bf16[128,2048]{1,0:T(8,128)(2,1)} fusion(f32[128,2,2048]{2,1,0:T(2,128)} %gather.7, pred[128,2]{1,0:T(8,128)(4,1)S(1)} %copy.33, f32[128,2]{1,0:T(8,128)S(1)} %copy.35), kind=kLoop, calls=%fused_computation.7 | loop fusion | flops 1310720 | bytes 2622720 | tf_op jit(solution)/shard_map/reduce_sum | solution.py:160
  (33 shorter events, 0.2 us)
Async XLA Ops:
  7.2 245.0 %copy-start = (bf16[512,2048]{1,0:T(8,128)(2,1)S(1)}, bf16[512,2048]{1,0:T(8,128)(2,1)}, u32[]{:S(2)}) copy-start(bf16[512,2048]{1,0:T(8,128)(2,1)} %param.18) | copy-start | bytes 6291460
  7.2 148.0 %all-gather.3.cloned.1.call-start = ((), (), s32[]{:S(2)}) async-start(), calls=%async_computation.8 | async-start | bytes 5242880 | tf_op jit(solution)/shard_map/all_gather | solution.py:140
  95.3 126.4 %all-gather.5.cloned.1.call-start = ((), (), s32[]{:S(2)}) async-start(), calls=%async_computation.10 | async-start | bytes 5242880 | tf_op jit(solution)/shard_map/all_gather | solution.py:140
  155.1 5.0 %copy-start.10 = (bf16[1,256,2048]{2,1,0:T(8,128)(2,1)S(1)}, bf16[1,256,2048]{2,1,0:T(8,128)(2,1)}, u32[]{:S(2)}) copy-start(bf16[1,256,2048]{2,1,0:T(8,128)(2,1)} %param.25) | copy-start | bytes 3145732
  155.1 146.7 %reduce-scatter.3.cloned.1.call-start = ((), (), s32[]{:S(2)}) async-start(), calls=%async_computation.9 | async-start | bytes 5242880 | tf_op jit(solution)/shard_map/reduce_scatter | solution.py:143
  169.2 0.7 copy-start.5
  169.2 1.1 copy-start.3
  172.2 49.4 %copy-start.9 = (bf16[1,2048,256]{2,1,0:T(8,128)(2,1)S(1)}, bf16[1,2048,256]{2,1,0:T(8,128)(2,1)}, u32[]{:S(2)}) copy-start(bf16[1,2048,256]{2,1,0:T(8,128)(2,1)} %param.23) | copy-start | bytes 3145732
  172.2 63.3 %all-to-all-start = ((bf16[4,128,2048]{2,1,0:T(8,128)(2,1)}), bf16[4,128,2048]{2,1,0:T(8,128)(2,1)}, u32[]{:S(2)}, u32[]{:S(2)}) async-start(bf16[4,128,2048]{2,1,0:T(8,128)(2,1)} %broadcast_in_dim.16), calls=%async_computation | async-start | bytes 4194304 | tf_op jit(solution)/shard_map/all_to_all | solution.py:11
  177.0 180.3 %reduce-scatter.5.cloned.1.call-start = ((), (), s32[]{:S(2)}) async-start(), calls=%async_computation.11 | async-start | bytes 5242880 | tf_op jit(solution)/shard_map/reduce_scatter | solution.py:143
  235.6 11.0 %copy-start.7 = (bf16[512]{0:T(512)(128)(2,1)S(1)}, bf16[512]{0:T(512)(128)(2,1)}, u32[]{:S(2)}) copy-start(bf16[512]{0:T(512)(128)(2,1)} %param.17) | copy-start | bytes 3076
  240.0 7.4 %copy-start.8 = (bf16[512,512]{1,0:T(8,128)(2,1)}, bf16[512,512]{1,0:T(8,128)(2,1)S(1)}, u32[]{:S(2)}) copy-start(bf16[512,512]{1,0:T(8,128)(2,1)S(1)} %get-tuple-element.9) | copy-start | bytes 1572868
  240.0 7.4 %collective-permute-start = (bf16[16,512]{1,0:T(8,128)(2,1)S(1)}, bf16[16,512]{1,0:T(8,128)(2,1)S(1)}, u32[]{:S(2)}, u32[]{:S(2)}) collective-permute-start(bf16[16,512]{1,0:T(8,128)(2,1)S(1)} %slice.70), channel_id=1, source_target_pairs={{0,4},{4,8},{8,12},{12,16},{16,20},{20,24},{24,28},{28,32},{32,36}... | collective-permute-start | bytes 49160 | tf_op jit(solution)/shard_map/ppermute | solution.py:30
  249.3 1.0 copy-start.1
  250.5 1.7 copy-start.2
  301.7 74.5 %copy-start.4 = (s32[128,2]{0,1:T(2,128)S(1)}, s32[128,2]{0,1:T(2,128)}, u32[]{:S(2)}) copy-start(s32[128,2]{0,1:T(2,128)} %param.21) | copy-start | bytes 3076
  301.7 75.0 %copy-start.6 = (f32[128,2]{0,1:T(2,128)S(1)}, f32[128,2]{0,1:T(2,128)}, u32[]{:S(2)}) copy-start(f32[128,2]{0,1:T(2,128)} %param.22) | copy-start | bytes 3076
  301.7 69.4 %all-to-all-start.3 = ((bf16[32,8,2048]{2,1,0:T(8,128)(2,1)}), bf16[32,8,2048]{2,1,0:T(8,128)(2,1)S(1)}, u32[]{:S(2)}, u32[]{:S(2)}) async-start(bf16[32,8,2048]{2,1,0:T(8,128)(2,1)} %bitcast.64), calls=%async_computation.4 | async-start | bytes 2097152 | tf_op jit(solution)/shard_map/all_to_all | solution.py:149
  371.2 60.7 %all-to-all-start.5 = ((bf16[32,8,2048]{2,1,0:T(8,128)(2,1)}), bf16[32,8,2048]{2,1,0:T(8,128)(2,1)}, u32[]{:S(2)}, u32[]{:S(2)}) async-start(bf16[32,8,2048]{2,1,0:T(8,128)(2,1)} %bitcast.65), calls=%async_computation.7 | async-start | bytes 2097152 | tf_op jit(solution)/shard_map/all_to_all | solution.py:149
Sparse Core Ops, SparseCore 0:
  95.4 46.6 all-gather.2
  155.2 66.3 all-gather.4
  224.2 77.4 reduce-scatter.2
  304.1 53.1 reduce-scatter.4
where the time goes:
time: 459 us; the launch traced here: 458 us
  blocking collectives  184 us (40%)
  waiting for transfers between devices  153 us (33%)
  matrix products  40.1 us (9%)
  starting transfers between devices  30.7 us (7%)
  other arithmetic  19.2 us (4%)
  local copies, waits for them, and re-layouts  16.9 us (4%)
  between operations  14.1 us (3%)
    all_to_all x2, blocking collectives, moved(): lax.all_to_all(group, axis, split_axis=split_dim, concat_axis=concat_dim,...  141 us
    all_to_all x2, waiting for transfers between devices, serve_sectioned(): lax.all_to_all(summed.reshape(sources, held, width).astype(jnp.bfloat16),...  66 us
    all_gather x2, waiting for transfers between devices, serve_sectioned(): lax.all_gather(flat, 'tp', axis=0, tiled=True)  44.4 us
    all_to_all x1, blocking collectives, sent_and_summed(): lax.all_to_all(tiles, axis, split_axis=0, concat_axis=0, tiled=True)  43.6 us
    reduce_scatter x2, waiting for transfers between devices, serve_sectioned(): lax.psum_scatter(jnp.dot(rows, down_weight[0], preferred_element_type=jnp...  41.5 us
    all_to_all x2, starting transfers between devices, serve_sectioned(): lax.all_to_all(summed.reshape(sources, held, width).astype(jnp.bfloat16),...  19 us
    dot_general x2, matrix products, serve_sectioned(): jnp.dot(rows, down_weight[0], preferred_element_type=jnp.float32)  18.6 us
    dot_general x2, matrix products, expert_hidden(): gate = jnp.dot(rows, w_gate, preferred_element_type=jnp.float32)  9.34 us
  transfers between devices with their start and end apart: 8, of which 5 were waited for; matrix products, arithmetic and copies ran while one was open for 10% of the time, Pallas kernels for 0%

commit v1 on v0

--- a/solution.py
+++ b/solution.py
@@ -133,28 +133,16 @@
     outgoing = jnp.dot(dispatch, expert_in, preferred_element_type=jnp.float32).astype(jnp.bfloat16)
     outgoing = outgoing.reshape(n_experts, capacity, width)
 
-    def serve_sectioned(arrived):
-        sources, held, _ = arrived.shape
-        flat = arrived.reshape(sources * held, width)
-        hidden = expert_hidden(
-            lax.all_gather(flat, "tp", axis=0, tiled=True), gate_weight[0], up_weight[0]
-        )
-        rows = lax.slice_in_dim(hidden, 0, sources * held * lax.axis_size("tp"), axis=0)
-        summed = lax.psum_scatter(
-            jnp.dot(rows, down_weight[0], preferred_element_type=jnp.float32).astype(jnp.bfloat16),
-            "tp",
-            scatter_dimension=0,
-            tiled=True,
-        ).astype(jnp.float32)
-        return lax.all_to_all(
-            summed.reshape(sources, held, width).astype(jnp.bfloat16),
-            "ep",
-            split_axis=0,
-            concat_axis=0,
-            tiled=True,
-        ).astype(jnp.float32)
-
-    expert_out = exchange_in_groups(outgoing, "ep", 0, 0, serve_sectioned, 1, 1)
+    gates = lax.all_gather(gate_weight[0], "tp", axis=0)
+    uppers = lax.all_gather(up_weight[0], "tp", axis=0)
+    downs = lax.all_gather(down_weight[0], "tp", axis=0)
+    arrived = lax.all_to_all(outgoing, "ep", 0, 0, tiled=True).reshape(n_experts * capacity, width)
+    made = jnp.zeros(arrived.shape, jnp.float32)
+    for block in range(gates.shape[0]):
+        hidden = expert_hidden(arrived, gates[block], uppers[block])
+        made = made + jnp.dot(hidden, downs[block], preferred_element_type=jnp.float32)
+    made = made.astype(jnp.bfloat16).reshape(n_experts, capacity, width)
+    expert_out = lax.all_to_all(made, "ep", 0, 0, tiled=True).astype(jnp.float32)
     flat_out = expert_out.reshape(n_experts * capacity, width)
     picked = jnp.take(flat_out, targets, axis=0).reshape(rows_here, top_k, width)
     expert_mix = jnp.sum(picked * shares[:, :, None], axis=1).astype(jnp.bfloat16)

time: 459 us -> 390 us (0.85); the launches traced: 458 us -> 382 us
  blocking collectives: 184 us -> 0 us
  starting transfers between devices: 30.7 us -> 83 us
  waiting for transfers between devices: 153 us -> 201 us
  matrix products: 40.1 us -> 52.2 us
    all_to_all x3 -> x0, blocking collectives: 184 us -> none  [the longest x2 141 us: moved(): lax.all_to_all(group, axis, split_axis=split_dim, concat_axis=concat_dim,...]
    ppermute x1, waiting for transfers between devices: 0.8 us -> 74.5 us  [shifted(): return lax.ppermute(value, axis, pairs)]
    all_to_all x2 -> x3, starting transfers between devices: 19 us -> 74 us  [the longest x1 53.6 us: local(): lax.all_to_all(outgoing, 'ep', 0, 0, tiled=True)]
    reduce_scatter x2 -> x0, waiting for transfers between devices: 41.5 us -> none  [serve_sectioned(): lax.psum_scatter(jnp.dot(rows, down_weight[0], preferred_element_type=jnp...]
    all_to_all x2 -> x3, waiting for transfers between devices: 66 us -> 99.7 us  [the longest x1 95.1 us: local(): lax.all_to_all(made, 'ep', 0, 0, tiled=True).astype(jnp.float32)]
    all_gather x2 -> x3, waiting for transfers between devices: 44.4 us -> 12.8 us  [the longest x1 12.8 us: local(): downs = lax.all_gather(down_weight[0], 'tp', axis=0)]
    all_to_all x1, waiting for transfers between devices: 0.01 us -> 11.6 us  [from_everyone(): lax.all_to_all(jnp.broadcast_to(value[None], (devices, *value.shape)), ax...]
    dot_general x2 -> x4, matrix products: 18.6 us -> 29 us  [local(): jnp.dot(hidden, downs[block], preferred_element_type=jnp.float32)]
  transfers between devices with their start and end apart: 8 -> 8, of which waited for: 5 -> 5; matrix products, arithmetic and copies ran while one was open for 10% -> 17% of each run, Pallas kernels for 0% -> 0%
where the time goes in v1:
time: 390 us; the launch traced here: 382 us
  waiting for transfers between devices  201 us (52%)
  starting transfers between devices  83 us (21%)
  matrix products  52.2 us (13%)
  local copies, waits for them, and re-layouts  16.8 us (4%)
  other arithmetic  15.5 us (4%)
  between operations  14.1 us (4%)
    all_to_all x1, waiting for transfers between devices, local(): lax.all_to_all(made, 'ep', 0, 0, tiled=True).astype(jnp.float32)  95.1 us
    ppermute x1, waiting for transfers between devices, shifted(): return lax.ppermute(value, axis, pairs)  74.5 us
    all_to_all x1, starting transfers between devices, local(): lax.all_to_all(outgoing, 'ep', 0, 0, tiled=True)  53.6 us
    dot_general x4, matrix products, local(): jnp.dot(hidden, downs[block], preferred_element_type=jnp.float32)  29 us
    all_to_all x1, starting transfers between devices, local(): lax.all_to_all(made, 'ep', 0, 0, tiled=True).astype(jnp.float32)  16.5 us
    all_gather x1, waiting for transfers between devices, local(): downs = lax.all_gather(down_weight[0], 'tp', axis=0)  12.8 us
    all_to_all x1, waiting for transfers between devices, from_everyone(): lax.all_to_all(jnp.broadcast_to(value[None], (devices, *value.shape)), ax...  11.6 us
    dot_general x4, matrix products, expert_hidden(): gate = jnp.dot(rows, w_gate, preferred_element_type=jnp.float32)  10.7 us
  transfers between devices with their start and end apart: 8, of which 5 were waited for; matrix products, arithmetic and copies ran while one was open for 17% of the time, Pallas kernels for 0%

profile of v1, /device:TPU:33, one launch (start us, length us, event | category | flops | bytes accessed | tf_op | source)
XLA Modules:
  0.0 382.5 jit_solution(17122592597432071071)
XLA Ops:
  7.2 0.0 copy-start
  7.2 0.0 copy-start.8
  7.2 0.0 copy-start.5
  7.2 0.1 all-gather.4.cloned.1.call-start
  7.3 0.7 all-gather.4.cloned.1.call-update
  8.0 0.1 all-gather.6.cloned.1.call-start
  8.1 0.7 all-gather.6.cloned.1.call-update
  8.8 0.0 copy-done.8
  8.8 0.2 fusion.9
  9.0 0.2 fusion.11
  9.3 1.6 broadcast_in_dim.16
  10.9 5.2 %all-to-all-start = ((bf16[4,128,2048]{2,1,0:T(8,128)(2,1)}), bf16[4,128,2048]{2,1,0:T(8,128)(2,1)}, u32[]{:S(2)}, u32[]{:S(2)}) async-start(bf16[4,128,2048]{2,1,0:T(8,128)(2,1)} %broadcast_in_dim.16), calls=%async_computation | async-start | bytes 4194304 | tf_op jit(solution)/shard_map/all_to_all | solution.py:11
  16.1 0.1 copy.34
  16.2 0.1 eq.55
  16.4 0.1 reshape.124
  16.6 0.6 reduce-window.6
  17.2 0.2 slice_reduce_fusion
  17.4 0.1 fusion.75
  17.5 0.1 reduce_sum.64
  17.6 0.1 copy.37
  17.7 0.1 fusion.58
  17.8 0.0 copy-done.6
  17.8 0.2 fusion.12
  18.0 2.1 convolution_convert_fusion
  20.1 11.6 %all-to-all-done = bf16[4,128,2048]{2,1,0:T(8,128)(2,1)} async-done(((bf16[4,128,2048]{2,1,0:T(8,128)(2,1)}), bf16[4,128,2048]{2,1,0:T(8,128)(2,1)}, u32[]{:S(2)}, u32[]{:S(2)}) %all-to-all-start) | async-done | bytes 2097184 | tf_op jit(solution)/shard_map/all_to_all | solution.py:11
  31.8 53.6 %all-to-all-start.2 = ((bf16[32,16,2048]{2,1,0:T(8,128)(2,1)}), bf16[32,16,2048]{2,1,0:T(8,128)(2,1)}, u32[]{:S(2)}, u32[]{:S(2)}) async-start(bf16[32,16,2048]{2,1,0:T(8,128)(2,1)} %bitcast.86), calls=%async_computation.2 | async-start | bytes 4194304 | tf_op jit(solution)/shard_map/all_to_all | solution.py:139
  85.4 0.1 all-gather.8.cloned.1.call-start
  85.5 0.7 all-gather.8.cloned.1.call-update
  86.2 0.0 copy-start.11
  86.2 4.5 %fusion.86 = (f32[512,512]{1,0:T(8,128)}, bf16[512,512]{1,0:T(8,128)(2,1)S(1)}) fusion(bf16[512,2048]{1,0:T(8,128)(2,1)} %bitcast, bf16[2048,512]{1,0:T(8,128)(2,1)} %param.15), kind=kOutput, calls=%fused_computation.123 | convolution fusion | flops 1074266112 | bytes 5767168 | tf_op jit(solution)/shard_map/dot_general | solution.py:89
  90.7 3.6 collective-permute-start
  94.3 74.5 %collective-permute-done = bf16[16,512]{1,0:T(8,128)(2,1)S(1)} collective-permute-done((bf16[16,512]{1,0:T(8,128)(2,1)S(1)}, bf16[16,512]{1,0:T(8,128)(2,1)S(1)}, u32[]{:S(2)}, u32[]{:S(2)}) %collective-permute-start) | collective-permute-done | bytes 16416 | tf_op jit(solution)/shard_map/ppermute | solution.py:30
  168.8 1.9 fusion.8
  170.7 0.1 slice_add_fusion.1
  170.8 1.0 copy-done.2
  171.8 0.1 slice_add_fusion
  172.0 1.6 fusion.85
  173.6 5.9 %convolution_convert_fusion.1 = bf16[512,2048]{1,0:T(8,128)(2,1)} fusion(bf16[512,2048]{1,0:T(8,128)(2,1)S(1)} %copy-done, f32[513,512]{1,0:T(8,128)} %get-tuple-element.5, f32[513,512]{1,0:T(8,128)} %get-tuple-element.4, f32[521,512]{1,0:T(8,128)} %copy-done.3, f32[525,512]{1,0:T(8,128)} %copy-done.2, f32[527,512]{1,0:T(8,128)S(1)} %fusion.8, ...), kind=kOutput, calls=%fused_computation.3 | convolution fusion | flops 1346895872 | bytes 10489860 | tf_op jit(solution)/shard_map/dot_general | solution.py:113
  179.6 4.6 %all-to-all-done.2 = bf16[32,16,2048]{2,1,0:T(8,128)(2,1)} async-done(((bf16[32,16,2048]{2,1,0:T(8,128)(2,1)}), bf16[32,16,2048]{2,1,0:T(8,128)(2,1)}, u32[]{:S(2)}, u32[]{:S(2)}) %all-to-all-start.2) | async-done | bytes 2097184 | tf_op jit(solution)/shard_map/all_to_all | solution.py:139
  184.1 3.9 %all-to-all-start.1 = ((bf16[4,128,2048]{2,1,0:T(8,128)(2,1)}), bf16[4,128,2048]{2,1,0:T(8,128)(2,1)S(1)}, u32[]{:S(2)}, u32[]{:S(2)}) async-start(bf16[4,128,2048]{2,1,0:T(8,128)(2,1)} %bitcast.87), calls=%async_computation.1 | async-start | bytes 4194304 | tf_op jit(solution)/shard_map/all_to_all | solution.py:41
  188.0 0.0 all-gather.4.cloned.1.call-done
  188.1 2.8 fusion.15
  190.8 0.4 copy-done.13
  191.2 2.3 fusion.17
  193.6 3.1 fusion.18
  196.7 12.8 %all-gather.8.cloned.1.call-done = bf16[4,256,2048]{2,1,0:T(8,128)(2,1)} async-done(((bf16[1,256,2048]{2,1,0:T(8,128)(2,1)}), bf16[4,256,2048]{2,1,0:T(8,128)(2,1)}) %all-gather.8.cloned.1.call-update) | async-done | bytes 4194320 | tf_op jit(solution)/shard_map/all_gather | solution.py:138
  209.5 6.6 %fusion.7 = f32[512,2048]{1,0:T(8,128)} fusion(bf16[512,2048]{1,0:T(8,128)(2,1)} %bitcast.5, bf16[4,256,2048]{2,1,0:T(8,128)(2,1)} %all-gather.8.cloned.1.call-done, bf16[4,2048,256]{2,1,0:T(8,128)(2,1)} %all-gather.6.cloned.1.call-done, f32[512,256]{1,0:T(8,128)} %fusion.18), kind=kOutput, calls=%fused_computation.23 | convolution fusion | flops 1074528256 | bytes 8912896 | tf_op jit(solution)/shard_map/dot_general | solution.py:143
  216.1 6.4 %fusion.6 = f32[512,2048]{1,0:T(8,128)} fusion(bf16[512,2048]{1,0:T(8,128)(2,1)} %bitcast.5, bf16[4,256,2048]{2,1,0:T(8,128)(2,1)} %all-gather.8.cloned.1.call-done, bf16[4,2048,256]{2,1,0:T(8,128)(2,1)} %all-gather.6.cloned.1.call-done, f32[512,256]{1,0:T(8,128)S(1)} %fusion.17), kind=kOutput, calls=%fused_computation.22 | convolution fusion | flops 1074528256 | bytes 8912896 | tf_op jit(solution)/shard_map/dot_general | solution.py:143
  222.5 2.6 fusion.16
  225.0 6.5 %fusion.5 = f32[512,2048]{1,0:T(8,128)} fusion(bf16[512,2048]{1,0:T(8,128)(2,1)} %bitcast.5, bf16[4,256,2048]{2,1,0:T(8,128)(2,1)} %all-gather.8.cloned.1.call-done, bf16[4,2048,256]{2,1,0:T(8,128)(2,1)} %all-gather.6.cloned.1.call-done, f32[512,256]{1,0:T(8,128)S(1)} %fusion.16), kind=kOutput, calls=%fused_computation.21 | convolution fusion | flops 1074528256 | bytes 8912896 | tf_op jit(solution)/shard_map/dot_general | solution.py:143
  231.5 9.5 %add_convert_fusion = bf16[512,2048]{1,0:T(8,128)(2,1)} fusion(f32[512,2048]{1,0:T(8,128)} %fusion.5, f32[512,2048]{1,0:T(8,128)} %fusion.7, f32[512,2048]{1,0:T(8,128)} %fusion.6, bf16[4,256,2048]{2,1,0:T(8,128)(2,1)} %all-gather.8.cloned.1.call-done, bf16[512,2048]{1,0:T(8,128)(2,1)} %bitcast.5, bf16[4,2048,256]{2,1,0:T(8,128)(2,1)} %all-gather.6.cloned.1.call-done, ...), kind=kOutput, calls=%fused_computation.1 | convolution fusion | flops 1078722560 | bytes 19398656 | tf_op jit(solution)/shard_map/dot_general | solution.py:143
  241.0 0.0 all-to-all-done.1
  241.0 1.3 copy-done.4
  242.4 16.5 %all-to-all-start.3 = ((bf16[32,16,2048]{2,1,0:T(8,128)(2,1)}), bf16[32,16,2048]{2,1,0:T(8,128)(2,1)S(1)}, u32[]{:S(2)}, u32[]{:S(2)}) async-start(bf16[32,16,2048]{2,1,0:T(8,128)(2,1)} %bitcast.18), calls=%async_computation.3 | async-start | bytes 4194304 | tf_op jit(solution)/shard_map/all_to_all | solution.py:145
  258.9 0.1 copy.39
  259.0 0.1 mul.130
  259.2 0.1 copy.40
  259.3 0.1 copy.38
  259.5 2.9 reduce_sum.62
  262.4 95.1 %all-to-all-done.3 = bf16[32,16,2048]{2,1,0:T(8,128)(2,1)S(1)} async-done(((bf16[32,16,2048]{2,1,0:T(8,128)(2,1)}), bf16[32,16,2048]{2,1,0:T(8,128)(2,1)S(1)}, u32[]{:S(2)}, u32[]{:S(2)}) %all-to-all-start.3) | async-done | bytes 2097184 | tf_op jit(solution)/shard_map/all_to_all | solution.py:145
  357.5 2.6 bitcast_convert_fusion
  360.1 5.8 %gather_fusion = f32[256,2048]{1,0:T(8,128)} fusion(f32[512,2048]{1,0:T(8,128)} %bitcast_convert_fusion, s32[1024]{0:T(1024)S(1)} %pad_clamp_fusion), kind=kCustom, calls=%fused_computation | custom fusion | bytes 4195328 | tf_op jit(solution)/shard_map/jit(_take)/gather | solution.py:147
  365.9 3.6 gather.7
  369.6 6.4 %multiply_reduce_fusion = bf16[128,2048]{1,0:T(8,128)(2,1)} fusion(f32[128,2,2048]{2,1,0:T(2,128)} %gather.7, pred[128,2]{1,0:T(8,128)(4,1)S(1)} %copy.38, f32[128,2]{1,0:T(8,128)S(1)} %copy.40), kind=kLoop, calls=%fused_computation.5 | loop fusion | flops 1310720 | bytes 2622720 | tf_op jit(solution)/shard_map/reduce_sum | solution.py:148
  (37 shorter events, 0.2 us)
Async XLA Ops:
  7.2 166.5 %copy-start = (bf16[512,2048]{1,0:T(8,128)(2,1)S(1)}, bf16[512,2048]{1,0:T(8,128)(2,1)}, u32[]{:S(2)}) copy-start(bf16[512,2048]{1,0:T(8,128)(2,1)} %param.18) | copy-start | bytes 6291460
  7.2 1.6 copy-start.8
  7.2 1.6 copy-start.5
  7.2 180.8 %all-gather.4.cloned.1.call-start = ((), (), s32[]{:S(2)}) async-start(), calls=%async_computation.4 | async-start | bytes 5242880 | tf_op jit(solution)/shard_map/all_gather | solution.py:136
  8.0 188.7 %all-gather.6.cloned.1.call-start = ((), (), s32[]{:S(2)}) async-start(), calls=%async_computation.5 | async-start | bytes 5242880 | tf_op jit(solution)/shard_map/all_gather | solution.py:137
  10.9 5.3 %copy-start.7 = (s32[128,2]{0,1:T(2,128)S(1)}, s32[128,2]{0,1:T(2,128)}, u32[]{:S(2)}) copy-start(s32[128,2]{0,1:T(2,128)} %param.21) | copy-start | bytes 3076
  10.9 5.7 %copy-start.9 = (bf16[2048]{0:T(1024)(128)(2,1)S(1)}, bf16[2048]{0:T(1024)(128)(2,1)}, u32[]{:S(2)}) copy-start(bf16[2048]{0:T(1024)(128)(2,1)} %param.20) | copy-start | bytes 12292
  10.9 6.9 %copy-start.6 = (bf16[128,2048]{1,0:T(8,128)(2,1)S(1)}, bf16[128,2048]{1,0:T(8,128)(2,1)}, u32[]{:S(2)}) copy-start(bf16[128,2048]{1,0:T(8,128)(2,1)} %param.19) | copy-start | bytes 1572868
  10.9 20.9 %all-to-all-start = ((bf16[4,128,2048]{2,1,0:T(8,128)(2,1)}), bf16[4,128,2048]{2,1,0:T(8,128)(2,1)}, u32[]{:S(2)}, u32[]{:S(2)}) async-start(bf16[4,128,2048]{2,1,0:T(8,128)(2,1)} %broadcast_in_dim.16), calls=%async_computation | async-start | bytes 4194304 | tf_op jit(solution)/shard_map/all_to_all | solution.py:11
  31.8 152.4 %all-to-all-start.2 = ((bf16[32,16,2048]{2,1,0:T(8,128)(2,1)}), bf16[32,16,2048]{2,1,0:T(8,128)(2,1)}, u32[]{:S(2)}, u32[]{:S(2)}) async-start(bf16[32,16,2048]{2,1,0:T(8,128)(2,1)} %bitcast.86), calls=%async_computation.2 | async-start | bytes 4194304 | tf_op jit(solution)/shard_map/all_to_all | solution.py:139
  85.4 124.0 %all-gather.8.cloned.1.call-start = ((), (), s32[]{:S(2)}) async-start(), calls=%async_computation.6 | async-start | bytes 5242880 | tf_op jit(solution)/shard_map/all_gather | solution.py:138
  86.2 8.1 %copy-start.11 = (bf16[512]{0:T(512)(128)(2,1)S(1)}, bf16[512]{0:T(512)(128)(2,1)}, u32[]{:S(2)}) copy-start(bf16[512]{0:T(512)(128)(2,1)} %param.17) | copy-start | bytes 3076
  90.7 78.1 %copy-start.12 = (bf16[512,512]{1,0:T(8,128)(2,1)}, bf16[512,512]{1,0:T(8,128)(2,1)S(1)}, u32[]{:S(2)}) copy-start(bf16[512,512]{1,0:T(8,128)(2,1)S(1)} %get-tuple-element.7) | copy-start | bytes 1572868
  90.7 78.1 %collective-permute-start = (bf16[16,512]{1,0:T(8,128)(2,1)S(1)}, bf16[16,512]{1,0:T(8,128)(2,1)S(1)}, u32[]{:S(2)}, u32[]{:S(2)}) collective-permute-start(bf16[16,512]{1,0:T(8,128)(2,1)S(1)} %slice.110), channel_id=1, source_target_pairs={{0,4},{4,8},{8,12},{12,16},{16,20},{20,24},{24,28},{28,32},{32,36}... | collective-permute-start | bytes 49160 | tf_op jit(solution)/shard_map/ppermute | solution.py:30
  170.8 1.0 copy-start.2
  172.0 1.7 copy-start.3
  184.1 56.9 %all-to-all-start.1 = ((bf16[4,128,2048]{2,1,0:T(8,128)(2,1)}), bf16[4,128,2048]{2,1,0:T(8,128)(2,1)S(1)}, u32[]{:S(2)}, u32[]{:S(2)}) async-start(bf16[4,128,2048]{2,1,0:T(8,128)(2,1)} %bitcast.87), calls=%async_computation.1 | async-start | bytes 4194304 | tf_op jit(solution)/shard_map/all_to_all | solution.py:41
  188.1 3.2 copy-start.13
  241.0 1.3 copy-start.4
  241.0 18.1 %copy-start.10 = (f32[128,2]{0,1:T(2,128)S(1)}, f32[128,2]{0,1:T(2,128)}, u32[]{:S(2)}) copy-start(f32[128,2]{0,1:T(2,128)} %param.22) | copy-start | bytes 3076
  242.4 115.2 %all-to-all-start.3 = ((bf16[32,16,2048]{2,1,0:T(8,128)(2,1)}), bf16[32,16,2048]{2,1,0:T(8,128)(2,1)S(1)}, u32[]{:S(2)}, u32[]{:S(2)}) async-start(bf16[32,16,2048]{2,1,0:T(8,128)(2,1)} %bitcast.18), calls=%async_computation.3 | async-start | bytes 4194304 | tf_op jit(solution)/shard_map/all_to_all | solution.py:145
  365.9 10.0 %copy-start.1 = (bf16[512,2048]{1,0:T(8,128)(2,1)S(1)}, bf16[512,2048]{1,0:T(8,128)(2,1)}, u32[]{:S(2)}) copy-start(bf16[512,2048]{1,0:T(8,128)(2,1)} %param.18) | copy-start | bytes 6291460
Sparse Core Ops, SparseCore 0:
  9.9 75.6 all-gather.3
  87.4 57.4 all-gather.5
  146.7 62.7 all-gather.7
